TPU v7x, 32 devices: a whole 2x2x4 slice. The times are simulated.
32 devices in a mesh: sp: 8 (over z, y), tp: 4 (over x, core).
Axes of the slice: x: 2, y: 2, z: 4, core: 2. Of those that a mesh axis runs over, the one named last changes fastest.
Arguments:
- tokens: bfloat16 [4096, 2048], P(('sp', 'tp')), may hold values from -6 to 6
- norm_gain: float32 [2048], replicated, may hold values from 0.25 to 5
- w_query_one: bfloat16 [2048, 512], P(None, 'tp'), may hold values from -0.21875 to 0.21875
- w_query_two: bfloat16 [2048, 512], P(None, 'tp'), may hold values from -0.21875 to 0.21875
- w_key_one: bfloat16 [2048, 512], P(None, 'tp'), may hold values from -0.125 to 0.125
- w_key_two: bfloat16 [2048, 512], P(None, 'tp'), may hold values from -0.125 to 0.125
- w_value: bfloat16 [2048, 1024], P(None, 'tp'), may hold values from -0.125 to 0.125
- mix_lambda: float32 [8], P('tp'), may hold values from 0.3 to 0.8
- head_gain: float32 [128], replicated, may hold values from 0.1 to 1.9
- w_ret_query: bfloat16 [2048, 512], P(None, 'tp'), may hold values from -0.125 to 0.125
- w_ret_key: bfloat16 [2048, 512], P(None, 'tp'), may hold values from -0.125 to 0.125
- w_ret_value: bfloat16 [2048, 1024], P(None, 'tp'), may hold values from -0.125 to 0.125
- retain_log: float32 [8, 4096], P('tp', 'sp'), may hold values from -1 to 0
- init_state: float32 [8, 64, 128], P('tp'), may hold values from -144 to 144
- w_out_diff: bfloat16 [1024, 2048], P('tp'), may hold values from -0.125 to 0.125
- w_out_ret: bfloat16 [1024, 2048], P('tp'), may hold values from -0.125 to 0.125
Outputs:
- mixed: bfloat16 [4096, 2048], P(('sp', 'tp'))
All inputs are finite; a program needn't handle non-finite values.
Results may differ from a plain program's by a relative error of at most 0.015.
The roundings to bfloat16 on the way count: a program that leaves them out, or rounds other values in their place, can miss the bound.
Values may be sent and summed in bfloat16 or wider, within the bound.
No kernel may reach another device: no remote copies, remote signals or barrier semaphores. Data moves between devices by JAX's collectives and lax.ppermute only.
A program may use at most 128 MiB of HBM per device.

v0:
```python
import math
import jax
import jax.numpy as jnp
from jax import lax
from jax.sharding import PartitionSpec as P

BLOCK = 256
NORM_EPS = 1e-06
HEAD_EPS = 1e-05
DIFF_SCALE = 0.8
HIGHEST = lax.Precision.HIGHEST


def prefix(x, axis, join, neutral):
    place = lax.axis_index(axis)
    gathered = jax.tree.map(
        lambda a, kind: lax.all_gather(a.astype(kind), axis), x, (jnp.bfloat16, jnp.bfloat16)
    )
    state = jax.tree.map(lambda a, e: jnp.zeros_like(a) + jnp.asarray(e, a.dtype), x, neutral)

    def one(turn, state):
        return join(
            state,
            jax.tree.map(
                lambda a, own: lax.dynamic_index_in_dim(a, turn, 0, False).astype(own.dtype),
                gathered,
                x,
            ),
        )

    return lax.fori_loop(0, place, one, state)


def head_norm(values):
    return values * lax.rsqrt(jnp.mean(values * values, axis=-1, keepdims=True) + HEAD_EPS)


def soft_update(running, query, keys, values, allowed):
    peak_old, denominator, weighted = running
    scores = jnp.einsum(
        "qhd,khd->hqk", query, keys, preferred_element_type=jnp.float32
    ) * query.shape[-1] ** (-0.5)
    scores = jnp.where(allowed[None], scores, -jnp.inf)
    peak_new = jnp.maximum(peak_old, jnp.max(scores, axis=-1))
    offset = jnp.where(jnp.isinf(peak_new), 0.0, peak_new)
    rescale = jnp.exp(peak_old - offset)
    shifted = jnp.exp(scores - offset[..., None])
    denominator = denominator * rescale + jnp.sum(shifted, axis=-1)
    weighted = weighted * rescale[..., None] + jnp.einsum(
        "hqk,khe->hqe", shifted.astype(jnp.bfloat16), values, preferred_element_type=jnp.float32
    )
    return (peak_new, denominator, weighted)


def on_device(
    tokens,
    norm_gain,
    w_query_one,
    w_query_two,
    w_key_one,
    w_key_two,
    w_value,
    mix_lambda,
    head_gain,
    w_ret_query,
    w_ret_key,
    w_ret_value,
    retain_log,
    init_state,
    w_out_diff,
    w_out_ret,
):
    key_width = w_query_one.shape[1]
    diff_heads = mix_lambda.shape[0]
    head_dim = key_width // diff_heads
    val_dim = head_gain.shape[0]
    value_width = w_value.shape[1]
    ret_heads = init_state.shape[0]
    ret_width = w_ret_query.shape[1]
    floats = tokens.astype(jnp.float32)
    normed = (
        floats * lax.rsqrt(jnp.mean(floats * floats, axis=-1, keepdims=True) + NORM_EPS) * norm_gain
    ).astype(jnp.bfloat16)
    weights = (
        w_query_one,
        w_query_two,
        w_key_one,
        w_key_two,
        w_value,
        w_ret_query,
        w_ret_key,
        w_ret_value,
    )
    portion = lax.all_gather(normed, "tp", axis=0, tiled=True)
    projected = jnp.concatenate(
        [
            jnp.dot(portion, weight, preferred_element_type=jnp.float32).astype(jnp.bfloat16)
            for weight in weights
        ],
        axis=1,
    )
    row_count = projected.shape[0]
    query_one = projected[:, :key_width].reshape(row_count, diff_heads, head_dim)
    query_two = projected[:, key_width : 2 * key_width].reshape(row_count, diff_heads, head_dim)
    key_pack = projected[:, 2 * key_width : 4 * key_width + value_width]
    ret_begin = 4 * key_width + value_width
    ret_query = projected[:, ret_begin : ret_begin + ret_width]
    ret_key = projected[:, ret_begin + ret_width : ret_begin + 2 * ret_width]
    ret_value = projected[:, ret_begin + 2 * ret_width :]
    nblocks = row_count // BLOCK

    def split_blocks(data, size):
        return data.reshape(nblocks, BLOCK, ret_heads, size).transpose(0, 2, 1, 3)

    block_query = split_blocks(ret_query, head_dim)
    block_key = split_blocks(ret_key, head_dim)
    block_value = split_blocks(ret_value, val_dim)
    log_blocks = retain_log.reshape(ret_heads, nblocks, BLOCK).transpose(1, 0, 2)
    sequence_index = jnp.arange(BLOCK, dtype=jnp.int32)
    causal = sequence_index[:, None] >= sequence_index[None, :]

    def ret_step(memory, inputs):
        query, keys, values, logs = inputs
        cumulative = jnp.cumsum(logs, axis=-1)
        gap_log = jnp.where(causal[None], cumulative[:, :, None] - cumulative[:, None, :], -jnp.inf)
        raw = jnp.einsum("hqd,hkd->hqk", query, keys, preferred_element_type=jnp.float32)
        decayed = (raw * head_dim ** (-0.5) * jnp.exp(gap_log)).astype(jnp.bfloat16)
        result = jnp.einsum("hqk,hke->hqe", decayed, values, preferred_element_type=jnp.float32)
        result = result + jnp.einsum(
            "hqd,hde->hqe",
            query.astype(jnp.float32) * jnp.exp(cumulative)[:, :, None],
            memory,
            precision=HIGHEST,
        )
        last_log = cumulative[:, -1:]
        key_scaled = (
            keys.astype(jnp.float32)
            * head_dim ** (-0.5)
            * jnp.exp(last_log - cumulative)[:, :, None]
        ).astype(jnp.bfloat16)
        memory = jnp.exp(last_log)[:, :, None] * memory + jnp.einsum(
            "hkd,hke->hde", key_scaled, values, preferred_element_type=jnp.float32
        )
        return (memory, result)

    zero_state = jnp.zeros((ret_heads, head_dim, val_dim), jnp.float32)
    local_state, local_out = lax.scan(
        ret_step, zero_state, (block_query, block_key, block_value, log_blocks)
    )
    span_log = jnp.sum(retain_log, axis=1)

    def chain_states(first_part, second_part):
        return (
            first_part[0] + second_part[0],
            first_part[1] * jnp.exp(second_part[0])[:, None, None] + second_part[1],
        )

    before_log, before_state = prefix(
        (span_log, local_state), "sp", chain_states, (jnp.zeros_like(span_log), zero_state)
    )
    carried = before_state + jnp.exp(before_log)[:, None, None] * init_state
    span_cumulative = jnp.cumsum(retain_log, axis=1)
    scaled_query = (
        ret_query.astype(jnp.float32).reshape(row_count, ret_heads, head_dim)
        * jnp.exp(span_cumulative).T[:, :, None]
    )
    ret_heads_out = local_out.transpose(1, 0, 2, 3).reshape(
        ret_heads, row_count, val_dim
    ) + jnp.einsum("thd,hde->hte", scaled_query, carried, precision=HIGHEST)
    ret_out = (
        head_norm(ret_heads_out)
        .transpose(1, 0, 2)
        .reshape(row_count, ret_heads * val_dim)
        .astype(jnp.bfloat16)
    )
    place = lax.axis_index("sp")
    query_pos = place * row_count + jnp.arange(row_count, dtype=jnp.int32)
    last_pos = place * row_count + row_count - 1

    def attend(running, key_block, begin_at):
        key_count = key_block.shape[0]
        keys_one = key_block[:, :key_width].reshape(key_count, diff_heads, head_dim)
        keys_two = key_block[:, key_width : 2 * key_width].reshape(key_count, diff_heads, head_dim)
        values = key_block[:, 2 * key_width :].reshape(key_count, diff_heads, val_dim)
        allowed = query_pos[:, None] >= (begin_at + jnp.arange(key_count, dtype=jnp.int32))[None, :]
        return (
            soft_update(running[0], query_one, keys_one, values, allowed),
            soft_update(running[1], query_two, keys_two, values, allowed),
        )

    empty_map = (
        jnp.full((diff_heads, row_count), -jnp.inf, jnp.float32),
        jnp.zeros((diff_heads, row_count), jnp.float32),
        jnp.zeros((diff_heads, row_count, val_dim), jnp.float32),
    )
    portion = lax.all_gather(key_pack, "sp", axis=0, tiled=True)
    key_count = portion.shape[0]
    stride = math.gcd(key_count, 512)

    def one_block(number, inner_state):
        first_pos = number * stride
        key_block = lax.dynamic_slice_in_dim(portion, number * stride, stride, 0)
        return lax.cond(
            first_pos <= last_pos,
            lambda kept: attend(kept, key_block, first_pos),
            lambda kept: kept,
            inner_state,
        )

    softmax_maps = lax.fori_loop(0, key_count // stride, one_block, (empty_map, empty_map))
    first_map, second_map = softmax_maps
    mixed_heads = (
        first_map[2] / first_map[1][..., None]
        - mix_lambda[:, None, None] * second_map[2] / second_map[1][..., None]
    )
    diff_out = (
        (head_norm(mixed_heads) * head_gain * DIFF_SCALE)
        .transpose(1, 0, 2)
        .reshape(row_count, diff_heads * val_dim)
        .astype(jnp.bfloat16)
    )
    return lax.psum_scatter(
        (
            jnp.dot(diff_out, w_out_diff, preferred_element_type=jnp.float32)
            + jnp.dot(ret_out, w_out_ret, preferred_element_type=jnp.float32)
        ).astype(jnp.bfloat16),
        "tp",
        scatter_dimension=0,
        tiled=True,
    )


def solution(mesh):
    in_specs = (
        P(("sp", "tp"), None),
        P(),
        P(None, "tp"),
        P(None, "tp"),
        P(None, "tp"),
        P(None, "tp"),
        P(None, "tp"),
        P("tp"),
        P(),
        P(None, "tp"),
        P(None, "tp"),
        P(None, "tp"),
        P("tp", "sp"),
        P("tp", None, None),
        P("tp", None),
        P("tp", None),
    )
    out_specs = P(("sp", "tp"), None)
    return jax.shard_map(
        on_device, mesh=mesh, in_specs=in_specs, out_specs=out_specs, check_vma=False
    )
```

profile of v0, /device:TPU:0, one launch (start us, length us, event | category | flops | bytes accessed | tf_op | source)
XLA Modules:
  0.0 263.3 jit_solution(5012526148714268753)
XLA Ops:
  6.5 1.3 fusion.56
  7.9 2.0 fusion.58
  11.6 23.1 %all-reduce = bf16[16]{0:T(256)(128)(2,1)S(1)} all-reduce(bf16[16]{0:T(256)(128)(2,1)S(1)} %dynamic-update-slice), channel_id=2, replica_groups=mesh['sp'=8,'tp'=4] {'sp'}, use_global_device_ids=true, to_apply=%add | all-reduce | flops 16 | bytes 64
  34.8 0.7 reshape.224
  37.1 2.8 %convolution_convert_fusion.1 = bf16[512,256]{0,1:T(8,128)(2,1)S(1)} fusion(bf16[512,2048]{1,0:T(8,128)(2,1)} %all-gather.5.cloned.1.call-done, bf16[2048,256]{1,0:T(8,128)(2,1)} %param.30), kind=kOutput, calls=%fused_computation.83 | convolution fusion | flops 537001984 | bytes 3407872 | tf_op jit(solution)/shard_map/dot_general | solution.py:97
  39.9 1.9 convolution_convert_fusion.6
  41.8 0.8 convolution_convert_fusion.7
  42.6 0.8 pad_maximum_fusion
  43.5 1.9 convolution_convert_fusion.2
  45.5 0.7 copy.65
  46.1 2.6 %convolution_convert_fusion = bf16[512,256]{1,0:T(8,128)(2,1)} fusion(bf16[512,2048]{1,0:T(8,128)(2,1)S(1)} %copy-done.2, bf16[2048,256]{1,0:T(8,128)(2,1)} %param.35), kind=kOutput, calls=%fused_computation.82 | convolution fusion | flops 537001984 | bytes 3407872 | tf_op jit(solution)/shard_map/dot_general | solution.py:97
  48.8 1.8 reshape.213
  50.5 1.7 copy.64
  52.2 1.7 convolution_convert_fusion.3
  54.1 0.7 copy.46
  54.8 14.2 %while.51 = (s32[]{:T(128)}, f32[2,64,128]{2,1,0:T(8,128)S(1)}, f32[2,2,256,128]{3,2,1,0:T(8,128)}, f32[2,2,256]{2,1,0:T(2,128)S(1)}, bf16[2,2,256,64]{2,3,1,0:T...) while((s32[]{:T(128)}, f32[2,64,128]{2,1,0:T(8,128)S(1)}, ...), condition=%wide.region_13.14_spmd.clone, body=%wide.region_10.13_spmd.clone.sunk | while | flops 110134280 | bytes 1677136 | solution.py:147
  56.6 1.4 fusion.109
  58.0 2.1 fusion.110
  60.1 0.6 exponential_bitcast_fusion.3
  60.8 1.1 convolution_add_fusion.6
  61.9 0.6 reduce-window.26
  63.7 1.4 fusion.109
  65.1 2.1 fusion.110
  67.3 0.6 exponential_bitcast_fusion.3
  67.9 1.1 convolution_add_fusion.6
  69.0 34.2 %all-gather.1 = bf16[16,64,128]{2,1,0:T(8,128)(2,1)} all-gather(bf16[2,64,128]{2,1,0:T(8,128)(2,1)S(1)} %convert_element_type.128), channel_id=3, replica_groups=mesh['sp'=8,'tp'=4] {'sp'}, dimensions={0}, use_global_device_ids=true | all-gather | bytes 294912 | tf_op jit(solution)/shard_map/all_gather | solution.py:17
  103.5 2.1 copy.47
  105.6 2.3 reshape.215
  107.8 1.8 multiply_reduce_fusion
  109.8 1.5 convolution_convert_fusion.5
  111.3 1.5 convolution_convert_fusion.4
  112.7 7.3 %all-gather.7.cloned.1.call-done = bf16[4096,512]{0,1:T(8,128)(2,1)} async-done(((bf16[512,512]{0,1:T(8,128)(2,1)}), bf16[4096,512]{0,1:T(8,128)(2,1)}) %all-gather.7.cloned.1.call-update) | async-done | bytes 4194320 | tf_op jit(solution)/shard_map/all_gather | solution.py:196
  120.1 0.8 broadcast_in_dim.88
  120.9 0.8 broadcast_in_dim.88.clone
  121.8 12.4 %while.50 = (s32[]{:T(128)}, f32[2,512]{1,0:T(2,128)S(1)}, f32[2,512]{1,0:T(2,128)S(1)}, f32[2,512,128]{2,1,0:T(8,128)}, f32[2,512]{1,0:T(2,128)S(1)}, /*index=5...) while((s32[]{:T(128)}, f32[2,512]{1,0:T(2,128)S(1)}, ...), condition=%wide.region_8.9_spmd.clone, body=%wide.region_1.8_spmd.clone.sunk | while | flops 410797056 | bytes 26628588 | solution.py:210
  121.8 12.0 %conditional.3 = ((f32[2,512]{1,0:T(2,128)S(1)}, f32[2,512]{1,0:T(2,128)S(1)}, f32[2,512,128]{2,1,0:T(8,128)}, f32[2,512]{1,0:T(2,128)S(1)}, f32[2,512]{1,0:T(2,128)S(1)}, /*index=5*/f32[2,512,128]{2,1,0:T(8,128)})) conditional(s32[]{:T(128)} %convert_element_type.180, (f32[2,512]{1,0:T(2,128)S(1)}, f32[2,512]{1,0:T(2,128)S(1)}, ...), branch_computations={%region_2.2_spmd, %region_3.7_spmd} | conditional | flops 410797056 | bytes 26626238 | solution.py:203
  121.8 1.0 fusion.63
  123.1 1.5 fusion.64
  124.7 0.6 fusion.65
  125.3 1.3 copy-done.1
  126.9 1.0 dynamic-slice.2
  127.9 3.1 %convolution_add_fusion = f32[2,512,128]{2,1,0:T(8,128)} fusion(bf16[512,2,128]{0,2,1:T(8,128)(2,1)S(1)} %bitcast.146, f32[2,512,512]{1,2,0:T(8,128)} %copy-done.1, f32[2,512]{1,0:T(2,128)S(1)} %get-tuple-element.549, f32[2,512,128]{2,1,0:T(8,128)} %get-tuple-element.368, f32[2,512]{1,0:T(2,128)S(1)} %get-tuple-element.548), kind=kOutput, calls=%fused_computation.10 | convolution fusion | flops 135528448 | bytes 3416064 | tf_op jit(solution)/shard_map/while/body/eval_jaxpr/cond/branch_1_fun/hqk,khe->hqe/dot_general | solution.py:49
  131.3 2.4 convolution_add_fusion.1
  134.2 1.2 copy.41
  135.4 1.2 copy.42
  137.1 0.7 fusion.66
  138.3 2.1 add_convert_fusion
  140.4 116.3 %reduce-scatter.2.cloned.1.call-done = bf16[128,2048]{1,0:T(8,128)(2,1)} async-done(((bf16[512,2048]{1,0:T(8,128)(2,1)}), bf16[128,2048]{1,0:T(8,128)(2,1)}) %reduce-scatter.2.cloned.1.call-update) | async-done | bytes 524304 | tf_op jit(solution)/shard_map/reduce_scatter | solution.py:222
  (118 shorter events, 8.0 us)
Async XLA Ops:
  6.5 130.5 %copy-start = (bf16[256,2048]{1,0:T(8,128)(2,1)S(1)}, bf16[256,2048]{1,0:T(8,128)(2,1)}, u32[]{:S(2)}) copy-start(bf16[256,2048]{1,0:T(8,128)(2,1)} %param.38) | copy-start | bytes 3145732
  6.5 3.5 %copy-start.16 = (u32[32]{0:T(128)S(1)}, u32[32]{0:T(128)}, u32[]{:S(2)}) copy-start(u32[32]{0:T(128)} %constant.133) | copy-start | bytes 388
  6.5 4.7 %copy-start.10 = (f32[2,512]{1,0:T(2,128)S(1)}, f32[2,512]{1,0:T(2,128)}, u32[]{:S(2)}) copy-start(f32[2,512]{1,0:T(2,128)} %param.36) | copy-start | bytes 12292
  6.5 30.5 %all-gather.5.cloned.1.call-start = ((), (), s32[]{:S(2)}) async-start(), calls=%async_computation.1 | async-start | bytes 2621440 | tf_op jit(solution)/shard_map/all_gather | solution.py:94
  9.9 110.2 %all-gather.7.cloned.1.call-start = ((), (), s32[]{:S(2)}) async-start(), calls=%async_computation.2 | async-start | bytes 4718592 | tf_op jit(solution)/shard_map/all_gather | solution.py:196
  37.1 2.8 %copy-start.2 = (bf16[512,2048]{1,0:T(8,128)(2,1)S(1)}, bf16[512,2048]{1,0:T(8,128)(2,1)}, u32[]{:S(2)}) copy-start(bf16[512,2048]{1,0:T(8,128)(2,1)} %all-gather.5.cloned.1.call-done) | copy-start | bytes 6291460
  39.8 1.9 copy-start.6
  43.5 213.2 %reduce-scatter.2.cloned.1.call-start = ((), (), s32[]{:S(2)}) async-start(), calls=%async_computation.3 | async-start | bytes 2621440 | tf_op jit(solution)/shard_map/reduce_scatter | solution.py:222
  45.4 3.4 %copy-start.3 = (bf16[512,128]{0,1:T(8,128)(2,1)}, bf16[512,128]{0,1:T(8,128)(2,1)S(1)}, u32[]{:S(2)}) copy-start(bf16[512,128]{0,1:T(8,128)(2,1)S(1)} %convolution_convert_fusion.2) | copy-start | bytes 393220
  56.0 0.5 copy-start.13
  63.1 0.5 copy-start.13
  69.0 38.8 %copy-start.4 = (bf16[512,128]{0,1:T(8,128)(2,1)S(1)}, bf16[512,128]{0,1:T(8,128)(2,1)}, u32[]{:S(2)}) copy-start(bf16[512,128]{0,1:T(8,128)(2,1)} %copy-done.3) | copy-start | bytes 393220
  69.0 38.8 %copy-start.11 = (f32[2,64,128]{2,1,0:T(8,128)S(1)}, f32[2,64,128]{2,1,0:T(8,128)}, u32[]{:S(2)}) copy-start(f32[2,64,128]{2,1,0:T(8,128)} %param.37) | copy-start | bytes 196612
  69.0 38.8 %copy-start.12 = (f32[1,2,4,128]{3,1,2,0:T(2,128)S(1)}, f32[1,2,4,128]{3,1,2,0:T(2,128)}, u32[]{:S(2)}) copy-start(f32[1,2,4,128]{3,1,2,0:T(2,128)} %copy.66) | copy-start | bytes 12292
  107.8 1.9 copy-start.7
  109.7 1.6 copy-start.8
  121.8 2.8 %copy-start.9 = (bf16[512,2,64]{0,2,1:T(8,128)(2,1)S(1)}, bf16[512,2,64]{0,2,1:T(8,128)(2,1)}, u32[]{:S(2)}) copy-start(bf16[512,2,64]{0,2,1:T(8,128)(2,1)} %get-tuple-element.366) | copy-start | bytes 393220 | tf_op jit(solution)/shard_map/while/body/eval_jaxpr/cond
  125.3 1.3 copy-start.1
  134.2 2.5 copy-start.14
  134.2 2.7 %copy-start.15 = (f32[128]{0:T(128)S(1)}, f32[128]{0:T(128)}, u32[]{:S(2)}) copy-start(f32[128]{0:T(128)} %param.32) | copy-start | bytes 1540
  137.0 1.2 copy-start.5
Sparse Core Ops, SparseCore 0:
  10.0 25.2 all-gather.4
  43.6 76.4 all-gather.6
  140.5 116.1 reduce-scatter.1
where the time goes:
time: 266 us; the launch traced here: 263 us
  waiting for transfers between devices  124 us (47%)
  blocking collectives  57.4 us (22%)
  matrix products  36.4 us (14%)
  local copies, waits for them, and re-layouts  22.5 us (8%)
  between operations  14.1 us (5%)
  other arithmetic  8.35 us (3%)
    reduce_scatter x1, waiting for transfers between devices, on_device(): lax.psum_scatter((jnp.dot(diff_out, w_out_diff, preferred_element_type=jn...  116 us
    all_gather x1, blocking collectives, prefix(): lax.all_gather(a.astype(kind), axis)  34.2 us
    unnamed x1, blocking collectives  23.1 us
    dot_general x8, matrix products, on_device(): jnp.dot(portion, weight, preferred_element_type=jnp.float32)  14.7 us
    all_gather x1, waiting for transfers between devices, on_device(): portion = lax.all_gather(key_pack, 'sp', axis=0, tiled=True)  7.34 us
    dot_general x2, matrix products, soft_update(): jnp.einsum('hqk,khe->hqe', shifted.astype(jnp.bfloat16), values, preferre...  5.55 us
  transfers between devices with their start and end apart: 3, of which 2 were waited for; matrix products, arithmetic and copies ran while one was open for 14% of the time, Pallas kernels for 0%

commit v1 on v0

--- a/solution.py
+++ b/solution.py
@@ -193,7 +193,9 @@
         jnp.zeros((diff_heads, row_count), jnp.float32),
         jnp.zeros((diff_heads, row_count, val_dim), jnp.float32),
     )
-    portion = lax.all_gather(key_pack, "sp", axis=0, tiled=True)
+    portion = jnp.concatenate(
+        lax.all_to_all(jnp.stack([key_pack] * lax.axis_size("sp")), "sp", 0, 0), axis=0
+    )
     key_count = portion.shape[0]
     stride = math.gcd(key_count, 512)
 

time: 266 us -> 281 us (1.056)
  blocking collectives: 57.4 us -> 107 us
  waiting for transfers between devices: 124 us -> 79.4 us
  local copies, waits for them, and re-layouts: 22.5 us -> 34.5 us
  matrix products: 36.4 us -> 31 us
  starting transfers between devices: 0.09 us -> 4.59 us
    all_gather x1, blocking collectives: 34.2 us -> 83.6 us  [prefix(): lax.all_gather(a.astype(kind), axis)]
    reduce_scatter x1, waiting for transfers between devices: 116 us -> 79.4 us  [on_device(): lax.psum_scatter((jnp.dot(diff_out, w_out_diff, preferred_element_type=jn...]
    unnamed x33 -> x36, local copies, waits for them, and re-layouts: 2.66 us -> 10.3 us
    all_gather x1 -> x0, waiting for transfers between devices: 7.34 us -> none  [on_device(): portion = lax.all_gather(key_pack, 'sp', axis=0, tiled=True)]
    all_to_all x0 -> x1, local copies, waits for them, and re-layouts: none -> 6.47 us  [on_device(): lax.all_to_all(jnp.stack([key_pack] * lax.axis_size('sp')), 'sp', 0, 0)]
    all_to_all x0 -> x1, starting transfers between devices: none -> 4.54 us  [on_device(): lax.all_to_all(jnp.stack([key_pack] * lax.axis_size('sp')), 'sp', 0, 0)]
    dot_general x2, matrix products: 5.55 us -> 1.42 us  [soft_update(): jnp.einsum('hqk,khe->hqe', shifted.astype(jnp.bfloat16), values, preferre...]
  transfers between devices with their start and end apart: 3 -> 3, of which waited for: 2 -> 1; matrix products, arithmetic and copies ran while one was open for 14% -> 14% of each run, Pallas kernels for 0% -> 0%
where the time goes in v1:
time: 281 us; the launch traced here: 279 us
  blocking collectives  107 us (38%)
  waiting for transfers between devices  79.4 us (28%)
  local copies, waits for them, and re-layouts  34.5 us (12%)
  matrix products  31 us (11%)
  between operations  14.4 us (5%)
  other arithmetic  7.59 us (3%)
  starting transfers between devices  4.59 us (2%)
    all_gather x1, blocking collectives, prefix(): lax.all_gather(a.astype(kind), axis)  83.6 us
    reduce_scatter x1, waiting for transfers between devices, on_device(): lax.psum_scatter((jnp.dot(diff_out, w_out_diff, preferred_element_type=jn...  79.4 us
    unnamed x1, blocking collectives  23.1 us
    dot_general x8, matrix products, on_device(): jnp.dot(portion, weight, preferred_element_type=jnp.float32)  14.5 us
    unnamed x36, local copies, waits for them, and re-layouts  10.3 us
    all_to_all x1, local copies, waits for them, and re-layouts, on_device(): lax.all_to_all(jnp.stack([key_pack] * lax.axis_size('sp')), 'sp', 0, 0)  6.47 us
  transfers between devices with their start and end apart: 3, of which 1 were waited for; matrix products, arithmetic and copies ran while one was open for 14% of the time, Pallas kernels for 0%

profile of v1, /device:TPU:0, one launch (start us, length us, event | category | flops | bytes accessed | tf_op | source)
XLA Modules:
  0.0 279.1 jit_solution(11218382077896090570)
XLA Ops:
  6.5 1.3 fusion.56
  7.9 2.0 fusion.58
  11.6 23.1 %all-reduce = bf16[16]{0:T(256)(128)(2,1)S(1)} all-reduce(bf16[16]{0:T(256)(128)(2,1)S(1)} %dynamic-update-slice), channel_id=2, replica_groups=mesh['sp'=8,'tp'=4] {'sp'}, use_global_device_ids=true, to_apply=%add | all-reduce | flops 16 | bytes 64
  34.7 0.7 reshape.230
  35.4 0.6 reduce-window.16
  36.4 0.6 copy.80
  37.1 2.6 convolution_convert_fusion.6
  39.7 1.9 convolution_convert_fusion.7
  41.6 0.8 convolution_convert_fusion.1
  42.4 2.3 stack.2
  44.8 4.5 %all-to-all-start = ((bf16[8,512,512]{1,2,0:T(8,128)(2,1)}), bf16[8,512,512]{1,2,0:T(8,128)(2,1)}, u32[]{:S(2)}, u32[]{:S(2)}) async-start(bf16[8,512,512]{1,2,0:T(8,128)(2,1)} %stack.2), calls=%async_computation | async-start | bytes 8388608 | tf_op jit(solution)/shard_map/all_to_all | solution.py:197
  49.4 1.9 convolution_convert_fusion.2
  51.3 0.7 copy.79
  51.9 2.4 convolution_convert_fusion.3
  54.3 1.0 copy.57
  55.4 0.7 reshape.218
  56.1 1.6 copy.60
  57.6 2.6 convolution_convert_fusion
  60.3 1.7 reshape.219
  62.0 1.7 copy.78
  63.7 13.0 %while.51 = (s32[]{:T(128)}, f32[2,64,128]{2,1,0:T(8,128)S(1)}, f32[2,2,256,128]{3,2,1,0:T(8,128)}, f32[2,2,256]{2,1,0:T(2,128)S(1)}, bf16[2,2,256,64]{2,3,1,0:T...) while((s32[]{:T(128)}, f32[2,64,128]{2,1,0:T(8,128)S(1)}, ...), condition=%wide.region_13.14_spmd.clone, body=%wide.region_10.13_spmd.clone.sunk | while | flops 110134280 | bytes 1678610 | solution.py:147
  63.7 0.6 reduce-window.26
  65.6 1.4 fusion.109
  67.0 2.2 fusion.110
  69.1 1.1 convolution_add_fusion.6
  70.2 0.6 reduce-window.26
  72.1 1.4 fusion.109
  73.5 2.1 fusion.110
  75.7 1.1 convolution_add_fusion.6
  76.8 2.1 copy.61
  78.9 2.3 reshape.221
  81.2 83.6 %all-gather.1 = bf16[16,64,128]{2,1,0:T(8,128)(2,1)} all-gather(bf16[2,64,128]{2,1,0:T(8,128)(2,1)S(1)} %convert_element_type.128), channel_id=3, replica_groups=mesh['sp'=8,'tp'=4] {'sp'}, dimensions={0}, use_global_device_ids=true | all-gather | bytes 294912 | tf_op jit(solution)/shard_map/all_gather | solution.py:17
  165.0 1.8 multiply_reduce_fusion
  167.0 0.8 convolution_convert_fusion.4
  167.9 1.5 convolution_convert_fusion.5
  169.4 6.5 %copy.53 = bf16[8,512,512]{2,1,0:T(8,128)(2,1)} copy(bf16[8,512,512]{1,2,0:T(8,128)(2,1)} %all-to-all-done) | data formatting | bytes 8388608 | tf_op jit(solution)/shard_map/all_to_all | solution.py:197
  175.9 6.4 %copy.54 = bf16[4096,512]{0,1:T(8,128)(2,1)} copy(bf16[4096,512]{1,0:T(8,128)(2,1)} %bitcast.149) | data formatting | bytes 8388608
  182.4 6.1 %while.50 = (s32[]{:T(128)}, f32[2,512]{1,0:T(2,128)S(1)}, f32[2,512]{1,0:T(2,128)S(1)}, f32[2,512,128]{2,1,0:T(8,128)S(1)}, f32[2,512]{1,0:T(2,128)S(1)}, /*ind...) while((s32[]{:T(128)}, f32[2,512]{1,0:T(2,128)S(1)}, ...), condition=%wide.region_8.9_spmd.clone, body=%wide.region_1.8_spmd.clone.sunk | while | flops 410797056 | bytes 17715636 | solution.py:212
  182.5 5.6 %conditional.3 = ((f32[2,512]{1,0:T(2,128)S(1)}, f32[2,512]{1,0:T(2,128)S(1)}, f32[2,512,128]{2,1,0:T(8,128)S(1)}, f32[2,512]{1,0:T(2,128)S(1)}, f32[2,512]{1,0:T(2,128)S(1)}, /*index=5*/f32[2,512,128]{2,1,0:T(8,128)S(1)})) conditional(s32[]{:T(128)} %convert_element_type.180, (f32[2,512]{1,0:T(2,128)S(1)}, f32[2,512]{1,0:T(2,128)S(1)}, ...), branch_computations={%region_2.2_spmd, %region_3.7_spmd} | conditional | flops 410797056 | bytes 17713286 | solution.py:205
  182.7 1.0 dynamic-slice.2
  183.7 1.0 fusion.63
  184.7 0.6 fusion.64
  185.4 0.6 fusion.65
  186.6 0.7 convolution_add_fusion.1
  187.4 0.7 convolution_add_fusion
  189.6 0.7 fusion.66
  190.8 2.1 add_convert_fusion
  192.9 79.4 %reduce-scatter.2.cloned.1.call-done = bf16[128,2048]{1,0:T(8,128)(2,1)} async-done(((bf16[512,2048]{1,0:T(8,128)(2,1)}), bf16[128,2048]{1,0:T(8,128)(2,1)}) %reduce-scatter.2.cloned.1.call-update) | async-done | bytes 524304 | tf_op jit(solution)/shard_map/reduce_scatter | solution.py:224
  (114 shorter events, 7.0 us)
Async XLA Ops:
  6.5 183.0 %copy-start = (bf16[256,2048]{1,0:T(8,128)(2,1)S(1)}, bf16[256,2048]{1,0:T(8,128)(2,1)}, u32[]{:S(2)}) copy-start(bf16[256,2048]{1,0:T(8,128)(2,1)} %param.38) | copy-start | bytes 3145732
  6.5 3.6 %copy-start.14 = (u32[32]{0:T(128)S(1)}, u32[32]{0:T(128)}, u32[]{:S(2)}) copy-start(u32[32]{0:T(128)} %constant.133) | copy-start | bytes 388
  6.5 3.4 %copy-start.8 = (f32[2,512]{1,0:T(2,128)S(1)}, f32[2,512]{1,0:T(2,128)}, u32[]{:S(2)}) copy-start(f32[2,512]{1,0:T(2,128)} %param.36) | copy-start | bytes 12292
  6.5 30.5 %all-gather.4.cloned.1.call-start = ((), (), s32[]{:S(2)}) async-start(), calls=%async_computation.2 | async-start | bytes 2621440 | tf_op jit(solution)/shard_map/all_gather | solution.py:94
  37.0 2.7 copy-start.1
  37.1 4.5 %copy-start.13 = (bf16[2048,256]{1,0:T(8,128)(2,1)S(1)}, bf16[2048,256]{1,0:T(8,128)(2,1)}, u32[]{:S(2)}) copy-start(bf16[2048,256]{1,0:T(8,128)(2,1)} %param.30) | copy-start | bytes 3145732
  44.8 124.7 %all-to-all-start = ((bf16[8,512,512]{1,2,0:T(8,128)(2,1)}), bf16[8,512,512]{1,2,0:T(8,128)(2,1)}, u32[]{:S(2)}, u32[]{:S(2)}) async-start(bf16[8,512,512]{1,2,0:T(8,128)(2,1)} %stack.2), calls=%async_computation | async-start | bytes 8388608 | tf_op jit(solution)/shard_map/all_to_all | solution.py:197
  49.3 223.0 %reduce-scatter.2.cloned.1.call-start = ((), (), s32[]{:S(2)}) async-start(), calls=%async_computation.3 | async-start | bytes 2621440 | tf_op jit(solution)/shard_map/reduce_scatter | solution.py:224
  51.2 9.0 %copy-start.2 = (bf16[512,128]{0,1:T(8,128)(2,1)}, bf16[512,128]{0,1:T(8,128)(2,1)S(1)}, u32[]{:S(2)}) copy-start(bf16[512,128]{0,1:T(8,128)(2,1)S(1)} %convolution_convert_fusion.2) | copy-start | bytes 393220
  76.7 88.3 %copy-start.3 = (bf16[512,128]{0,1:T(8,128)(2,1)S(1)}, bf16[512,128]{0,1:T(8,128)(2,1)}, u32[]{:S(2)}) copy-start(bf16[512,128]{0,1:T(8,128)(2,1)} %copy-done.2) | copy-start | bytes 393220
  76.8 88.3 %copy-start.9 = (f32[2,64,128]{2,1,0:T(8,128)S(1)}, f32[2,64,128]{2,1,0:T(8,128)}, u32[]{:S(2)}) copy-start(f32[2,64,128]{2,1,0:T(8,128)} %param.37) | copy-start | bytes 196612
  76.8 88.3 %copy-start.10 = (f32[1,2,4,128]{3,1,2,0:T(2,128)S(1)}, f32[1,2,4,128]{3,1,2,0:T(2,128)}, u32[]{:S(2)}) copy-start(f32[1,2,4,128]{3,1,2,0:T(2,128)} %copy.80) | copy-start | bytes 12292
  165.0 2.0 copy-start.5
  166.9 1.0 copy-start.6
  175.9 6.6 %copy-start.7 = (bf16[512,128]{0,1:T(8,128)(2,1)S(1)}, bf16[512,128]{0,1:T(8,128)(2,1)}, u32[]{:S(2)}) copy-start(bf16[512,128]{0,1:T(8,128)(2,1)} %convolution_convert_fusion.5) | copy-start | bytes 393220
  188.5 0.7 copy-start.11
  188.6 0.9 copy-start.12
  189.5 1.2 copy-start.4
Sparse Core Ops, SparseCore 0:
  10.1 25.2 all-gather.3
  193.0 79.2 reduce-scatter.1
